TPU v7x, 32 devices: a whole 2x2x4 slice. The times are simulated.
32 devices in a mesh: sp: 4 (over y, x), tp: 8 (over z, core).
Axes of the slice: x: 2, y: 2, z: 4, core: 2. Of those that a mesh axis runs over, the one named last changes fastest.
Arguments:
- mix_in: bfloat16 [4096, 2048], P('sp', 'tp'), may hold values from -8 to 8
- gate_in: bfloat16 [4096, 2048], P('sp', 'tp'), may hold values from -6 to 6
- conv_w: float32 [4, 2048], P(None, 'tp'), may hold values from -3 to 3
- conv_b: float32 [2048], P('tp'), may hold values from -3 to 3
- decay_param: float32 [2, 2048], P(None, 'tp')
- recur_gate: float32 [2, 32, 64, 64], P(None, 'tp'), may hold values from -0.75 to 0.75
- recur_bias: float32 [2, 2048], P(None, 'tp'), may hold values from -4 to 4
- input_gate: float32 [2, 32, 64, 64], P(None, 'tp'), may hold values from -0.75 to 0.75
- input_bias: float32 [2, 2048], P(None, 'tp'), may hold values from -4 to 4
- residual: bfloat16 [4096, 2048], P(('sp', 'tp')), may hold values from -6 to 6
- out_proj: bfloat16 [2048, 2048], replicated, may hold values from -0.125 to 0.125
- norm_gain: float32 [3, 2048], replicated, may hold values from 0.1 to 1.9
- routes: int32 [4096, 2], P('sp'), may hold values from 0 to 15, all different within a row; in each aligned block of 128 rows (0 to 127, 128 to 255, ...) at most 32 rows name the same one
- route_wt: float32 [4096, 2], P('sp'), may hold values from 0.1 to 1
- exp_gate: bfloat16 [16, 2048, 1024], P('sp', None, 'tp'), may hold values from -0.125 to 0.125
- exp_up: bfloat16 [16, 2048, 1024], P('sp', None, 'tp'), may hold values from -0.125 to 0.125
- exp_down: bfloat16 [16, 1024, 2048], P('sp', 'tp'), may hold values from -0.1875 to 0.1875
Outputs:
- final: bfloat16 [4096, 2048], P(('sp', 'tp'))
Inputs may be any that keep to these rules, and one draw needn't show every extreme that they name: `routes`: in each aligned block of 128 tokens (the rows of one device in the expert layer) no expert is named more than 32 times, and in some block some expert exactly 32 times; a token's 2 experts differ.
All inputs are finite; a program needn't handle non-finite values.
Results may differ from a plain program's by a relative error of at most 0.008.
Values may be sent and summed in bfloat16 or wider, within the bound.
A program may use at most 128 MiB of HBM per device.

v0:
```python
import functools

import jax
import jax.numpy as jnp
from jax import lax
from jax.experimental import pallas as pl
from jax.experimental.pallas import tpu as pltpu
from jax.sharding import PartitionSpec as P

EPSILON = 1e-06
HIGHEST_MODE = lax.Precision.HIGHEST
MESH = pl.DeviceIdType.MESH
HALO = 16
SUB = 8


def norm_rows(values, gain):
    floats = values.astype(jnp.float32)
    return floats * lax.rsqrt(jnp.mean(floats * floats, axis=-1, keepdims=True) + EPSILON) * gain


def slot_table(route_rows, experts, capacity):
    row_count, top_count = route_rows.shape
    flattened = route_rows.reshape(row_count * top_count)
    matches = flattened[:, None] == jnp.arange(experts, dtype=jnp.int32)[None, :]
    order = jnp.arange(row_count * top_count, dtype=jnp.int32)
    before = (order[None, :] < order[:, None]).astype(jnp.bfloat16)
    earlier_hits = jnp.dot(
        before, matches.astype(jnp.bfloat16), preferred_element_type=jnp.float32
    )
    position = jnp.sum(jnp.where(matches, earlier_hits, 0.0), axis=1).astype(jnp.int32)
    return (flattened * capacity + position).reshape(row_count, top_count)


def weight_table(slots, route_weights, total_slots):
    matches = slots[..., None] == jnp.arange(total_slots, dtype=jnp.int32)
    return jnp.sum(jnp.where(matches, route_weights[..., None], 0.0), axis=-2)


def one_minus_exp(y):
    series = -y * (1.0 + y * (1.0 / 2) * (1.0 + y * (1.0 / 3) * (1.0 + y * 0.25 * (1.0 + y * 0.2))))
    return jnp.where(y > -0.1, series, 1.0 - jnp.exp(y))


def split_f32(x):
    high = x.astype(jnp.bfloat16)
    return high, (x - high.astype(jnp.float32)).astype(jnp.bfloat16)


def tile_scan(a, b, reverse):
    row = lax.broadcasted_iota(jnp.int32, a.shape, 1)
    step = 1
    while step < SUB:
        shift = SUB - step if reverse else step
        keep = row < SUB - step if reverse else row >= step
        a_prev = jnp.where(keep, pltpu.roll(a, shift, 1), 1.0)
        b_prev = jnp.where(keep, pltpu.roll(b, shift, 1), 0.0)
        b = b + a * b_prev
        a = a * a_prev
        step *= 2
    return a, b


def mixer_kernel(
    dims,
    mix_ref, gate_ref, cw_ref, cb_ref, soft_ref, rg_ref, rb_ref, ig_ref, ib_ref,
    res_ref, gain_ref, slots_ref, op_hbm, eg_hbm, eu_hbm, ed_hbm,
    stream_ref, arrived_hbm, gf_hbm, uf_hbm, df_hbm,
    xp, wh, wl, af, bf, ab, bb, mixed, tok, op, proj, outgoing, halo, summ, ends,
    bg, bu, bd,
    op_sem, own_sem, halo_send, halo_recv, sum_send, sum_recv,
    mix_send, mix_recv, dis_send, dis_recv, z_send, z_recv, c_send, c_recv,
):
    S, T, L, G = dims
    seq, C = mix_ref.shape
    rows, D = res_ref.shape
    slots = outgoing.shape[0]
    cap = slots // (S * L)
    heads, hd = rg_ref.shape[1], rg_ref.shape[2]
    F = eg_hbm.shape[2]
    sp = lax.axis_index("sp")
    tp = lax.axis_index("tp")
    q = tp // G
    g = lax.rem(tp, G)

    def place_of(dq, dg):
        return lax.rem(q + dq, L) * G + lax.rem(g + dg, G)

    op_copy = pltpu.make_async_copy(op_hbm, op, op_sem)
    op_copy.start()
    own_in = [
        pltpu.make_async_copy(h.at[q], v, own_sem.at[i])
        for i, (h, v) in enumerate(((eg_hbm, bg), (eu_hbm, bu), (ed_hbm, bd)))
    ]
    for c in own_in:
        c.start()

    barrier = pltpu.get_barrier_semaphore()
    greeted = 0
    for ds in range(S):
        for dq in range(L):
            for dg in range(G):
                if (ds or dq or dg) and (ds == 0 or dg == 0):
                    pl.semaphore_signal(
                        barrier, inc=1,
                        device_id=(lax.rem(sp + ds, S), place_of(dq, dg)),
                        device_id_type=MESH,
                    )
                    greeted += 1
    pl.semaphore_wait(barrier, greeted)

    def remote(src, dst, send, recv, sp_to, tp_to):
        return pltpu.make_async_remote_copy(
            src_ref=src, dst_ref=dst, send_sem=send, recv_sem=recv,
            device_id=(sp_to, tp_to), device_id_type=MESH,
        )

    to_next = remote(mix_ref.at[pl.ds(seq - HALO, HALO)], halo.at[0], halo_send.at[0],
                     halo_recv.at[0], lax.rem(sp + 1, S), tp)
    to_prev = remote(mix_ref.at[pl.ds(0, HALO)], halo.at[1], halo_send.at[1],
                     halo_recv.at[1], lax.rem(sp + S - 1, S), tp)
    to_next.start()
    to_prev.start()

    def full_slot(ref, axis, place):
        if len(ref.shape) == 3:
            return ref.at[place]
        start = pl.multiple_of(place * F, F)
        return ref.at[:, pl.ds(start, F)] if axis else ref.at[pl.ds(start, F), :]

    tensors = ((eg_hbm, gf_hbm, 1), (eu_hbm, uf_hbm, 1), (ed_hbm, df_hbm, 0))

    def z_copies(dq):
        return [
            remote(src.at[lax.rem(q + dq, L)], full_slot(dst, axis, tp), z_send.at[dq, i],
                   z_recv.at[dq, i], sp, place_of(dq, 0))
            for i, (src, dst, axis) in enumerate(tensors)
        ]

    def core_copies(dq, i, own):
        src, dst, axis = tensors[i]
        origin = place_of(L - dq, 0)
        at = full_slot(dst, axis, origin)
        return [
            remote(own if own is not None else at, at, c_send.at[dq, dg, i], c_recv.at[dq, dg, i],
                   sp, place_of(0, dg))
            for dg in range(1, G)
        ]

    far = [dq for dq in range(1, L) if min(dq, L - dq) > 1]
    near = [dq for dq in range(1, L) if min(dq, L - dq) == 1]
    z_all = {dq: z_copies(dq) for dq in range(1, L)}
    for i in range(3):
        for dq in near:
            z_all[dq][i].start()
    own_out, core_all = [], {}
    for i, (src, dst, axis) in enumerate(tensors):
        core_all[0, i] = core_copies(0, i, src.at[q])
        for c in core_all[0, i]:
            c.start()
    for i, (buf, (src, dst, axis)) in enumerate(zip((bg, bu, bd), tensors)):
        own_in[i].wait()
        c = pltpu.make_async_copy(buf, full_slot(dst, axis, tp), own_sem.at[3 + i])
        c.start()
        own_out.append(c)

    wh[...] = jnp.zeros_like(wh)
    wl[...] = jnp.zeros_like(wl)
    for k, ref in enumerate((rg_ref, ig_ref)):
        for sense in range(2):
            for h in range(heads):
                high, low = split_f32(ref[sense, h])
                col = (2 * sense + k) * C + h * hd
                wh[h * hd : (h + 1) * hd, col : col + hd] = high
                wl[h * hd : (h + 1) * hd, col : col + hd] = low
    xp[SUB : SUB + seq, :] = mix_ref[...].astype(jnp.float32)
    to_next.wait()
    to_prev.wait()
    tail = halo[0].astype(jnp.float32)[HALO - SUB : HALO]
    head = halo[1].astype(jnp.float32)[0:SUB]
    xp[0:SUB, :] = jnp.where(sp > 0, tail, 0.0)
    xp[SUB + seq : 2 * SUB + seq, :] = jnp.where(sp < S - 1, head, 0.0)

    R = min(128, seq)

    def gates(n, _):
        base = pl.multiple_of(n * R, R)
        window = xp[pl.ds(base, R + 2 * SUB), :]
        conv = cb_ref[...] + window[SUB - 2 : SUB - 2 + R] * cw_ref[0:1]
        for tap in range(1, cw_ref.shape[0]):
            conv = conv + window[SUB - 2 + tap : SUB - 2 + tap + R] * cw_ref[tap : tap + 1]
        high, low = split_f32(conv)
        for sense, (a_ref, b_ref) in enumerate(((af, bf), (ab, bb))):
            cols = slice(2 * sense * C, (2 * sense + 2) * C)
            pre = jnp.dot(high, wh[:, cols], preferred_element_type=jnp.float32)
            pre = pre + jnp.dot(low, wh[:, cols], preferred_element_type=jnp.float32)
            pre = pre + jnp.dot(high, wl[:, cols], preferred_element_type=jnp.float32)
            recur = jax.nn.sigmoid(pre[:, :C] + rb_ref[sense : sense + 1])
            inp = jax.nn.sigmoid(pre[:, C:] + ib_ref[sense : sense + 1])
            log_a = -8.0 * recur * soft_ref[sense : sense + 1]
            a = jnp.exp(log_a)
            b = jnp.sqrt(one_minus_exp(2.0 * log_a)) * (inp * conv)
            a, b = tile_scan(
                a.reshape(R // SUB, SUB, C), b.reshape(R // SUB, SUB, C), sense == 1
            )
            a_ref[pl.ds(base, R), :] = a.reshape(R, C)
            b_ref[pl.ds(base, R), :] = b.reshape(R, C)
        return 0

    lax.fori_loop(0, seq // R, gates, 0)

    tiles = seq // SUB

    def carry(t, held):
        sf, pf, sb, pb = held
        at = pl.ds(pl.multiple_of(t * SUB, SUB), SUB)
        a = af[at, :]
        s = bf[at, :] + a * sf
        p = a * pf
        af[at, :] = p
        bf[at, :] = s
        back = pl.ds(pl.multiple_of((tiles - 1 - t) * SUB, SUB), SUB)
        a = ab[back, :]
        s2 = bb[back, :] + a * sb
        p2 = a * pb
        ab[back, :] = p2
        bb[back, :] = s2
        return s[SUB - 1 : SUB], p[SUB - 1 : SUB], s2[0:1], p2[0:1]

    zero, one = jnp.zeros((1, C), jnp.float32), jnp.ones((1, C), jnp.float32)
    sf, pf, sb, pb = lax.fori_loop(0, tiles, carry, (zero, one, zero, one), unroll=4)
    summ[0:1, :] = sf
    summ[1:2, :] = pf
    summ[2:3, :] = sb
    summ[3:4, :] = pb
    sums = [
        remote(summ, ends.at[ds - 1], sum_send.at[ds - 1], sum_recv.at[ds - 1],
               lax.rem(sp + ds, S), tp)
        for ds in range(1, S)
    ]
    for c in sums:
        c.start()
    for c in sums:
        c.wait()
    fe, be = zero, zero
    for ds in range(S - 1, 0, -1):
        fe = jnp.where(sp >= ds, ends[ds - 1, 1:2, :] * fe + ends[ds - 1, 0:1, :], fe)
    for ds in range(1, S):
        be = jnp.where(sp + S - ds < S, ends[ds - 1, 3:4, :] * be + ends[ds - 1, 2:3, :], be)

    def join(n, _):
        at = pl.ds(pl.multiple_of(n * R, R), R)
        state = (bf[at, :] + af[at, :] * fe) + (bb[at, :] + ab[at, :] * be)
        mixed[at, :] = (state * jax.nn.gelu(gate_ref[at, :].astype(jnp.float32))).astype(
            jnp.bfloat16
        )
        return 0

    lax.fori_loop(0, seq // R, join, 0)

    def block_rows(place):
        return mixed.at[pl.ds(pl.multiple_of(place * rows, rows), rows), :]

    columns = pl.ds(pl.multiple_of(tp * C, C), C)
    moves = []
    for dq in range(L):
        for dg in range(G):
            if dq or dg:
                k = dq * G + dg
                to = place_of(dq, dg)
                moves.append(remote(block_rows(to), tok.at[:, columns], mix_send.at[k],
                                    mix_recv.at[k], sp, to))
    for c in moves:
        c.start()
    own_move = pltpu.make_async_copy(block_rows(tp), tok.at[:, columns], own_sem.at[6])
    own_move.start()
    for dq in far:
        for c in z_all[dq]:
            c.start()
    op_copy.wait()
    own_move.wait()
    for c in moves:
        c.wait()

    def project(n, _):
        cols = pl.ds(pl.multiple_of(n * 256, 256), 256)
        proj[:, cols] = (
            jnp.dot(tok[...], op[:, cols], preferred_element_type=jnp.float32)
            .astype(jnp.bfloat16)
        )
        return 0

    lax.fori_loop(0, D // 256, project, 0)
    part = 32

    def norms(n, _):
        at = pl.ds(pl.multiple_of(n * part, part), part)
        s = (
            res_ref[at, :].astype(jnp.float32) + norm_rows(proj[at, :], gain_ref[0:1, :])
        ).astype(jnp.bfloat16)
        stream_ref[at, :] = s
        tok[at, :] = norm_rows(s, gain_ref[1:2, :]).astype(jnp.bfloat16)
        return 0

    lax.fori_loop(0, rows // part, norms, 0)
    slot_id = lax.broadcasted_iota(jnp.int32, (slots, rows), 0)
    hit = slot_id == slots_ref[0:1, :]
    for k in range(1, slots_ref.shape[0]):
        hit = hit | (slot_id == slots_ref[k : k + 1, :])
    selector = jnp.where(hit, 1.0, 0.0).astype(jnp.bfloat16)

    def dispatch(n, _):
        cols = pl.ds(pl.multiple_of(n * 256, 256), 256)
        outgoing[:, cols] = (
            jnp.dot(selector, tok[:, cols], preferred_element_type=jnp.float32)
            .astype(jnp.bfloat16)
        )
        return 0

    lax.fori_loop(0, D // 256, dispatch, 0)
    sends = []
    mine = sp * L + q
    for ds in range(S):
        for dq in range(L):
            sp_to, q_to = lax.rem(sp + ds, S), lax.rem(q + dq, L)
            src = outgoing.at[pl.ds(pl.multiple_of((sp_to * L + q_to) * cap, cap), cap), :]
            if ds or dq:
                k = ds * L + dq
                sends.append(remote(src, arrived_hbm.at[mine], dis_send.at[k], dis_recv.at[k],
                                    sp_to, q_to * G + g))
            else:
                sends.append(pltpu.make_async_copy(src, arrived_hbm.at[mine], own_sem.at[7]))
    for c in sends:
        c.start()
    for dq in near + far:
        for i in range(3):
            z_all[dq][i].wait_recv()
            core_all[dq, i] = core_copies(dq, i, None)
            for c in core_all[dq, i]:
                c.start()
    for c in sends:
        c.wait()
    for dq in range(1, L):
        for c in z_all[dq]:
            c.wait_send()
    for c in own_out:
        c.wait()
    for group in core_all.values():
        for c in group:
            c.wait()


def return_kernel(dims, rows_hbm, back_hbm, own_sem, send, recv):
    S, T, L, G = dims
    sp = lax.axis_index("sp")
    tp = lax.axis_index("tp")
    q = tp // G
    g = lax.rem(tp, G)
    barrier = pltpu.get_barrier_semaphore()
    peers = [
        (ds, dq, lax.rem(sp + ds, S), lax.rem(q + dq, L))
        for ds in range(S) for dq in range(L) if ds or dq
    ]
    for ds, dq, sp_to, q_to in peers:
        pl.semaphore_signal(
            barrier, inc=1, device_id=(sp_to, q_to * G + g), device_id_type=MESH
        )
    pl.semaphore_wait(barrier, len(peers))
    mine = sp * L + q
    copies = [
        pltpu.make_async_remote_copy(
            src_ref=rows_hbm.at[sp_to * L + q_to], dst_ref=back_hbm.at[mine],
            send_sem=send.at[ds * L + dq], recv_sem=recv.at[ds * L + dq],
            device_id=(sp_to, q_to * G + g), device_id_type=MESH,
        )
        for ds, dq, sp_to, q_to in peers
    ]
    copies.append(pltpu.make_async_copy(rows_hbm.at[mine], back_hbm.at[mine], own_sem))
    for c in copies:
        c.start()
    for c in copies:
        c.wait()


def on_device(
    mix_in, gate_in, conv_w, conv_b, decay_param, recur_gate, recur_bias, input_gate, input_bias,
    residual, out_proj, norm_gain, routes, route_wt, exp_gate, exp_up, exp_down,
):
    S, T = lax.axis_size("sp"), lax.axis_size("tp")
    L, D, F = exp_gate.shape
    G = T // L
    dims = (S, T, L, G)
    seq, C = mix_in.shape
    rows = residual.shape[0]
    top_count = routes.shape[1]
    experts = L * S
    cap = 2 * rows * top_count // experts
    total_slots = experts * cap
    own_start = lax.axis_index("tp") * rows
    own_routes = lax.dynamic_slice_in_dim(routes, own_start, rows, 0)
    own_weights = lax.dynamic_slice_in_dim(route_wt, own_start, rows, 0)
    own_slots = slot_table(own_routes, experts, cap)
    soft = jax.nn.softplus(-decay_param)
    wide = F % 128 == 0
    vmem = pl.BlockSpec(memory_space=pltpu.VMEM)
    hbm = pl.BlockSpec(memory_space=pltpu.MemorySpace.HBM)
    b16, f32 = jnp.bfloat16, jnp.float32
    dma = pltpu.SemaphoreType.DMA
    sds = jax.ShapeDtypeStruct
    up_shape = (D, T * F) if wide else (T, D, F)
    down_shape = (T * F, D) if wide else (T, F, D)
    stream, arrived, gate_full, up_full, down_full = pl.pallas_call(
        functools.partial(mixer_kernel, dims),
        out_shape=(
            sds((rows, D), b16), sds((experts, cap, D), b16),
            sds(up_shape, b16), sds(up_shape, b16), sds(down_shape, b16),
        ),
        in_specs=[vmem] * 12 + [hbm] * 4,
        out_specs=(vmem, hbm, hbm, hbm, hbm),
        scratch_shapes=[
            pltpu.VMEM((seq + 2 * SUB, C), f32),
            pltpu.VMEM((C, 4 * C), b16),
            pltpu.VMEM((C, 4 * C), b16),
            pltpu.VMEM((seq, C), f32), pltpu.VMEM((seq, C), f32),
            pltpu.VMEM((seq, C), f32), pltpu.VMEM((seq, C), f32),
            pltpu.VMEM((seq, C), b16),
            pltpu.VMEM((rows, T * C), b16),
            pltpu.VMEM(out_proj.shape, b16),
            pltpu.VMEM((rows, D), b16),
            pltpu.VMEM((total_slots, D), b16),
            pltpu.VMEM((2, HALO, C), b16),
            pltpu.VMEM((SUB, C), f32),
            pltpu.VMEM((S - 1, SUB, C), f32),
            pltpu.VMEM((D, F), b16), pltpu.VMEM((D, F), b16), pltpu.VMEM((F, D), b16),
            dma, dma((8,)),
            dma((2,)), dma((2,)),
            dma((S - 1,)), dma((S - 1,)),
            dma((T,)), dma((T,)),
            dma((experts,)), dma((experts,)),
            dma((L, 3)), dma((L, 3)),
            dma((L, G, 3)), dma((L, G, 3)),
        ],
        compiler_params=pltpu.CompilerParams(
            collective_id=0, has_side_effects=True, vmem_limit_bytes=56 * 1024 * 1024
        ),
    )(
        mix_in, gate_in, conv_w, conv_b.reshape(1, C), soft, recur_gate, recur_bias, input_gate,
        input_bias, residual, norm_gain, own_slots.T, out_proj, exp_gate, exp_up, exp_down,
    )
    flat = arrived.reshape(total_slots, D)
    if wide:
        gate_act = jnp.dot(flat, gate_full, preferred_element_type=f32)
        up_act = jnp.dot(flat, up_full, preferred_element_type=f32)
    else:
        gate_act = jnp.einsum("md,tdf->mtf", flat, gate_full, preferred_element_type=f32)
        up_act = jnp.einsum("md,tdf->mtf", flat, up_full, preferred_element_type=f32)
    hidden = (jax.nn.silu(gate_act) * up_act).astype(b16).reshape(total_slots, T * F)
    out_rows = jnp.dot(
        hidden, down_full.reshape(T * F, D), preferred_element_type=f32
    ).astype(b16)
    returned = pl.pallas_call(
        functools.partial(return_kernel, dims),
        out_shape=sds((experts, cap, D), b16),
        in_specs=[hbm],
        out_specs=hbm,
        scratch_shapes=[dma, dma((experts,)), dma((experts,))],
        compiler_params=pltpu.CompilerParams(collective_id=1, has_side_effects=True),
    )(out_rows.reshape(experts, cap, D))
    values = returned.reshape(total_slots, D).astype(f32)
    own_table = weight_table(own_slots, own_weights, total_slots)
    mixture = jnp.dot(own_table, values, precision=HIGHEST_MODE).astype(b16)
    mixture = lax.optimization_barrier(mixture)
    return (stream.astype(f32) + norm_rows(mixture, norm_gain[2])).astype(b16)


def solution(mesh):
    return jax.shard_map(
        on_device,
        mesh=mesh,
        in_specs=(
            P("sp", "tp"),
            P("sp", "tp"),
            P(None, "tp"),
            P("tp"),
            P(None, "tp"),
            P(None, "tp", None, None),
            P(None, "tp"),
            P(None, "tp", None, None),
            P(None, "tp"),
            P(("sp", "tp"), None),
            P(),
            P(),
            P("sp", None),
            P("sp", None),
            P("sp", None, "tp"),
            P("sp", None, "tp"),
            P("sp", "tp", None),
        ),
        out_specs=P(("sp", "tp"), None),
        check_vma=False,
    )
```

profile of v0, /device:TPU:0, one launch (start us, length us, event | category | flops | bytes accessed | tf_op | source)
XLA Modules:
  0.0 276.9 jit_solution(2506260236939900451)
XLA Ops:
  0.0 0.0 copy-start
  0.0 0.7 constant_dynamic-slice_fusion.1
  0.7 0.1 copy.24
  0.8 0.1 eq.28
  1.0 0.2 fusion
  1.2 0.1 convert_element_type.31
  1.3 0.1 copy.25
  1.4 1.2 multiply_add_fusion
  2.6 1.3 compare_select_fusion.soft_ref
  3.9 200.3 %shard_map.163 = (bf16[128,2048]{1,0:T(8,128)(2,1)}, bf16[16,32,2048]{2,1,0:T(8,128)(2,1)}, bf16[2048,1024]{1,0:T(8,128)(2,1)}, bf16[2048,1024]{1,0:T(8,128)(2,1)}, bf16[1024,2048]{1,0:T(8,128)(2,1)}) custom-call(bf16[1024,256]{1,0:T(8,128)(2,1)} %mix_ref.1, bf16[1024,256]{1,0:T(8,128)(2,1)} %gate_ref.1, f32[4,256]{1,0:T(4,128)} %cw_ref.1, ...), custom_call_target="tpu_custom_call" | custom-call | tf_op jit(solution)/shard_map/pallas_call | solution.py:412
  204.2 0.0 copy-start.3
  204.2 6.6 %fusion.7 = f32[512,1024]{1,0:T(8,128)} fusion(bf16[512,2048]{1,0:T(8,128)(2,1)} %bitcast.18, bf16[2048,1024]{1,0:T(8,128)(2,1)} %get-tuple-element.12), kind=kOutput, calls=%fused_computation.22 | convolution fusion | flops 2147483648 | bytes 8388608 | tf_op jit(solution)/shard_map/dot_general | solution.py:452
  210.9 0.0 copy-done.3
  210.9 10.1 %convolution_convert_fusion = bf16[512,2048]{1,0:T(8,128)(2,1)} fusion(bf16[1024,2048]{1,0:T(8,128)(2,1)} %get-tuple-element.14, f32[512,1024]{1,0:T(8,128)} %fusion.7, bf16[512,2048]{1,0:T(8,128)(2,1)S(1)} %bitcast.19, bf16[2048,1024]{1,0:T(8,128)(2,1)} %get-tuple-element.13), kind=kOutput, calls=%fused_computation | convolution fusion | flops 4299161600 | bytes 14680064 | tf_op jit(solution)/shard_map/dot_general | solution.py:458
  220.9 0.0 copy-start.2
  220.9 51.2 %shard_map.164 = bf16[16,32,2048]{2,1,0:T(8,128)(2,1)} custom-call(bf16[16,32,2048]{2,1,0:T(8,128)(2,1)} %bitcast.14), custom_call_target="tpu_custom_call" | custom-call | tf_op jit(solution)/shard_map/pallas_call | solution.py:461
  272.1 0.0 copy-start.1
  272.1 0.0 copy-done
  272.1 0.0 copy-done.2
  272.1 0.1 select_reduce_fusion
  272.3 2.6 convolution_convert_fusion.1
  274.9 0.2 fusion.1
  275.1 0.8 slice.3
  275.9 0.0 copy-done.1
  275.9 1.1 fusion.4
  (3 shorter events, 0.0 us)
Async XLA Ops:
  0.0 272.1 %copy-start = (f32[1024,2]{0,1:T(2,128)S(1)}, f32[1024,2]{0,1:T(2,128)}, u32[]{:S(2)}) copy-start(f32[1024,2]{0,1:T(2,128)} %param.30) | copy-start | bytes 24580
  204.2 6.6 %copy-start.3 = (bf16[16,32,2048]{2,1,0:T(8,128)(2,1)S(1)}, bf16[16,32,2048]{2,1,0:T(8,128)(2,1)}, u32[]{:S(2)}) copy-start(bf16[16,32,2048]{2,1,0:T(8,128)(2,1)} %get-tuple-element.11) | copy-start | bytes 6291460
  220.9 51.2 %copy-start.2 = (s32[128,2]{0,1:T(2,128)S(1)}, s32[128,2]{0,1:T(2,128)}, u32[]{:S(2)}) copy-start(s32[128,2]{0,1:T(2,128)} %multiply_add_fusion) | copy-start | bytes 3076
  272.1 3.8 %copy-start.1 = (bf16[128,2048]{1,0:T(8,128)(2,1)S(1)}, bf16[128,2048]{1,0:T(8,128)(2,1)}, u32[]{:S(2)}) copy-start(bf16[128,2048]{1,0:T(8,128)(2,1)} %get-tuple-element.10) | copy-start | bytes 1572868
where the time goes:
time: 277 us
  Pallas kernels  251 us (91%)
  matrix products  19.5 us (7%)
  other arithmetic  3.92 us (1%)
    pallas_call x1, Pallas kernels, on_device(): pl.pallas_call(functools.partial(mixer_kernel, dims), out_shape=(sds((row...  200 us
    pallas_call x1, Pallas kernels, on_device(): pl.pallas_call(functools.partial(return_kernel, dims), out_shape=sds((exp...  51.2 us
    dot_general x1, matrix products, on_device(): jnp.dot(hidden, down_full.reshape(T * F, D), preferred_element_type=f32)  10.1 us
    dot_general x1, matrix products, on_device(): gate_act = jnp.dot(flat, gate_full, preferred_element_type=f32)  6.63 us

commit v1 on v0

v1 whole, which is shorter than its diff:
```python
import functools

import jax
import jax.numpy as jnp
from jax import lax
from jax.experimental import pallas as pl
from jax.experimental.pallas import tpu as pltpu
from jax.sharding import PartitionSpec as P

EPSILON = 1e-06
HIGHEST_MODE = lax.Precision.HIGHEST
MESH = pl.DeviceIdType.MESH
HALO = 16
SUB = 8
LAG = 2
RING = 2


def norm_rows(values, gain):
    floats = values.astype(jnp.float32)
    return floats * lax.rsqrt(jnp.mean(floats * floats, axis=-1, keepdims=True) + EPSILON) * gain


def slot_tables(routes, route_wt, dims, rows, cap, local):
    S, T, L, Z = dims
    top = routes.shape[1]
    pair = 2 * rows
    flat = routes.reshape(T, rows * top).T
    wanted = jnp.arange(S, dtype=jnp.int32) * L + local
    matches = flat[:, :, None] == wanted
    order = jnp.arange(rows * top, dtype=jnp.int32)
    before = (order[None, :] < order[:, None]).astype(jnp.bfloat16)
    earlier = jnp.dot(
        before, matches.reshape(rows * top, T * S).astype(jnp.bfloat16),
        preferred_element_type=jnp.float32,
    ).reshape(rows * top, T, S)
    core = (jnp.arange(T, dtype=jnp.int32) % 2)[:, None]
    slot = (jnp.arange(S, dtype=jnp.int32) * 2 + core) * cap
    ids = jnp.where(matches, earlier.astype(jnp.int32) + slot + 1, 0).sum(axis=2) - 1
    ids = ids.reshape(rows, top, T)
    by_slot = ids.transpose(2, 0, 1).reshape(Z, pair, top)
    weights = route_wt.reshape(Z, pair, top)
    return by_slot.transpose(0, 2, 1), by_slot, weights


def one_minus_exp(y):
    series = -y * (1.0 + y * (1.0 / 2) * (1.0 + y * (1.0 / 3) * (1.0 + y * 0.25 * (1.0 + y * 0.2))))
    return jnp.where(y > -0.1, series, 1.0 - jnp.exp(y))


def split_f32(x):
    high = x.astype(jnp.bfloat16)
    return high, (x - high.astype(jnp.float32)).astype(jnp.bfloat16)


def tile_scan(a, b, reverse):
    row = lax.broadcasted_iota(jnp.int32, a.shape, 1)
    step = 1
    while step < SUB:
        shift = SUB - step if reverse else step
        keep = row < SUB - step if reverse else row >= step
        a_prev = jnp.where(keep, pltpu.roll(a, shift, 1), 1.0)
        b_prev = jnp.where(keep, pltpu.roll(b, shift, 1), 0.0)
        b = b + a * b_prev
        a = a * a_prev
        step *= 2
    return a, b


def layer_kernel(
    dims,
    mix_ref, gate_ref, cw_ref, cb_ref, soft_ref, rg_ref, rb_ref, ig_ref, ib_ref,
    res_ref, gain_ref, sel_ref, comb_ref, wt_ref, op_hbm, eg_hbm, eu_hbm, ed_hbm,
    out_ref,
    xp, wh, wl, af, bf, ab, bb, mixed, tok, op, proj, halo, summ, ends,
    wg, wu, wd, hid, stream, gath, outg, arr, back, prem, zrec, pbuf,
    op_sem, own_sem, halo_send, halo_recv, sum_send, sum_recv,
    mix_send, mix_recv, w_send, w_recv, ga_send, ga_recv, d2_send, d2_recv,
    dis_send, dis_recv, ret_send, ret_recv, pd_send, pd_recv, zs_send, zs_recv,
):
    S, T, L, Z = dims
    seq, C = mix_ref.shape
    rows, D = res_ref.shape
    two_cap = arr.shape[2]
    slots = S * two_cap
    heads, hd = rg_ref.shape[1], rg_ref.shape[2]
    F = eg_hbm.shape[2]
    sp = lax.axis_index("sp")
    tp = lax.axis_index("tp")
    z = lax.div(tp, 2)
    g = lax.rem(tp, 2)
    local = lax.rem(tp, L)
    part_base = tp - local
    partner = tp + 1 - 2 * g

    op_copy = pltpu.make_async_copy(op_hbm, op, op_sem)
    op_copy.start()

    barrier = pltpu.get_barrier_semaphore()
    greeted = 0
    for ds in range(S):
        for dt in range(T):
            if (ds == 0) != (dt == 0):
                pl.semaphore_signal(
                    barrier, inc=1,
                    device_id=(lax.rem(sp + ds, S), lax.rem(tp + dt, T)),
                    device_id_type=MESH,
                )
                greeted += 1
    pl.semaphore_wait(barrier, greeted)

    def remote(src, dst, send, recv, sp_to, tp_to):
        return pltpu.make_async_remote_copy(
            src_ref=src, dst_ref=dst, send_sem=send, recv_sem=recv,
            device_id=(sp_to, tp_to), device_id_type=MESH,
        )

    to_next = remote(mix_ref.at[pl.ds(seq - HALO, HALO)], halo.at[0], halo_send.at[0],
                     halo_recv.at[0], lax.rem(sp + 1, S), tp)
    to_prev = remote(mix_ref.at[pl.ds(0, HALO)], halo.at[1], halo_send.at[1],
                     halo_recv.at[1], lax.rem(sp + S - 1, S), tp)
    to_next.start()
    to_prev.start()

    tensors = ((eg_hbm, wg, 1), (eu_hbm, wu, 1), (ed_hbm, wd, 0))

    def chunk(ref, axis, place):
        if len(ref.shape) == 3:
            return ref.at[place]
        if ref.shape[axis] == F:
            return ref
        start = pl.multiple_of(place * F, F)
        return ref.at[:, pl.ds(start, F)] if axis else ref.at[pl.ds(start, F), :]

    def weight_copy(i, d):
        src, dst, axis = tensors[i]
        to = lax.rem(local + d, L)
        return remote(src.at[to], chunk(dst, axis, local), w_send.at[d - 1, i],
                      w_recv.at[d - 1, i], sp, part_base + to)

    own_weights = [
        pltpu.make_async_copy(src.at[local], chunk(dst, axis, local), own_sem.at[i])
        for i, (src, dst, axis) in enumerate(tensors)
    ]
    for c in own_weights:
        c.start()
    for i in range(2):
        for d in range(1, L):
            weight_copy(i, d).start()

    wh[...] = jnp.zeros_like(wh)
    wl[...] = jnp.zeros_like(wl)
    for k, ref in enumerate((rg_ref, ig_ref)):
        for sense in range(2):
            for h in range(heads):
                high, low = split_f32(ref[sense, h])
                col = (2 * sense + k) * C + h * hd
                wh[h * hd : (h + 1) * hd, col : col + hd] = high
                wl[h * hd : (h + 1) * hd, col : col + hd] = low
    xp[SUB : SUB + seq, :] = mix_ref[...].astype(jnp.float32)
    to_next.wait()
    to_prev.wait()
    tail = halo[0].astype(jnp.float32)[HALO - SUB : HALO]
    head = halo[1].astype(jnp.float32)[0:SUB]
    xp[0:SUB, :] = jnp.where(sp > 0, tail, 0.0)
    xp[SUB + seq : 2 * SUB + seq, :] = jnp.where(sp < S - 1, head, 0.0)

    R = min(128, seq)

    def gates(n, _):
        base = pl.multiple_of(n * R, R)
        window = xp[pl.ds(base, R + 2 * SUB), :]
        conv = cb_ref[...] + window[SUB - 2 : SUB - 2 + R] * cw_ref[0:1]
        for tap in range(1, cw_ref.shape[0]):
            conv = conv + window[SUB - 2 + tap : SUB - 2 + tap + R] * cw_ref[tap : tap + 1]
        high, low = split_f32(conv)
        for sense, (a_ref, b_ref) in enumerate(((af, bf), (ab, bb))):
            cols = slice(2 * sense * C, (2 * sense + 2) * C)
            pre = jnp.dot(high, wh[:, cols], preferred_element_type=jnp.float32)
            pre = pre + jnp.dot(low, wh[:, cols], preferred_element_type=jnp.float32)
            pre = pre + jnp.dot(high, wl[:, cols], preferred_element_type=jnp.float32)
            recur = jax.nn.sigmoid(pre[:, :C] + rb_ref[sense : sense + 1])
            inp = jax.nn.sigmoid(pre[:, C:] + ib_ref[sense : sense + 1])
            log_a = -8.0 * recur * soft_ref[sense : sense + 1]
            a = jnp.exp(log_a)
            b = jnp.sqrt(one_minus_exp(2.0 * log_a)) * (inp * conv)
            a, b = tile_scan(
                a.reshape(R // SUB, SUB, C), b.reshape(R // SUB, SUB, C), sense == 1
            )
            a_ref[pl.ds(base, R), :] = a.reshape(R, C)
            b_ref[pl.ds(base, R), :] = b.reshape(R, C)
        return 0

    lax.fori_loop(0, seq // R, gates, 0)

    tiles = seq // SUB

    def carry(t, held):
        sf, pf, sb, pb = held
        at = pl.ds(pl.multiple_of(t * SUB, SUB), SUB)
        a = af[at, :]
        s = bf[at, :] + a * sf
        p = a * pf
        af[at, :] = p
        bf[at, :] = s
        back = pl.ds(pl.multiple_of((tiles - 1 - t) * SUB, SUB), SUB)
        a = ab[back, :]
        s2 = bb[back, :] + a * sb
        p2 = a * pb
        ab[back, :] = p2
        bb[back, :] = s2
        return s[SUB - 1 : SUB], p[SUB - 1 : SUB], s2[0:1], p2[0:1]

    zero, one = jnp.zeros((1, C), jnp.float32), jnp.ones((1, C), jnp.float32)
    sf, pf, sb, pb = lax.fori_loop(0, tiles, carry, (zero, one, zero, one), unroll=4)
    summ[0:1, :] = sf
    summ[1:2, :] = pf
    summ[2:3, :] = sb
    summ[3:4, :] = pb
    sums = [
        remote(summ, ends.at[ds - 1], sum_send.at[ds - 1], sum_recv.at[ds - 1],
               lax.rem(sp + ds, S), tp)
        for ds in range(1, S)
    ]
    for c in sums:
        c.start()
    for c in sums:
        c.wait()
    fe, be = zero, zero
    for ds in range(S - 1, 0, -1):
        fe = jnp.where(sp >= ds, ends[ds - 1, 1:2, :] * fe + ends[ds - 1, 0:1, :], fe)
    for ds in range(1, S):
        be = jnp.where(sp + S - ds < S, ends[ds - 1, 3:4, :] * be + ends[ds - 1, 2:3, :], be)

    def join(n, _):
        at = pl.ds(pl.multiple_of(n * R, R), R)
        state = (bf[at, :] + af[at, :] * fe) + (bb[at, :] + ab[at, :] * be)
        mixed[at, :] = (state * jax.nn.gelu(gate_ref[at, :].astype(jnp.float32))).astype(
            jnp.bfloat16
        )
        return 0

    lax.fori_loop(0, seq // R, join, 0)

    def block_rows(place):
        return mixed.at[pl.ds(pl.multiple_of(place * rows, rows), rows), :]

    columns = pl.ds(pl.multiple_of(tp * C, C), C)
    moves = []
    for dt in range(1, T):
        to = lax.rem(tp + dt, T)
        moves.append(remote(block_rows(to), tok.at[:, columns], mix_send.at[dt],
                            mix_recv.at[dt], sp, to))
    for c in moves:
        c.start()
    own_move = pltpu.make_async_copy(block_rows(tp), tok.at[:, columns], own_sem.at[6])
    own_move.start()
    op_copy.wait()
    own_move.wait()
    for c in moves:
        c.wait()

    def project(n, _):
        cols = pl.ds(pl.multiple_of(n * 256, 256), 256)
        proj[:, cols] = (
            jnp.dot(tok[...], op[:, cols], preferred_element_type=jnp.float32)
            .astype(jnp.bfloat16)
        )
        return 0

    lax.fori_loop(0, D // 256, project, 0)
    part = 32

    def norms(n, _):
        at = pl.ds(pl.multiple_of(n * part, part), part)
        s = (
            res_ref[at, :].astype(jnp.float32) + norm_rows(proj[at, :], gain_ref[0:1, :])
        ).astype(jnp.bfloat16)
        stream[at, :] = s
        gath[tp, at, :] = norm_rows(s, gain_ref[1:2, :]).astype(jnp.bfloat16)
        return 0

    lax.fori_loop(0, rows // part, norms, 0)
    wide = min(256, D)

    def chip_at(j):
        low = jnp.minimum(z, Z - 1 - z)
        d = lax.div(j + 1, 2)
        near = jnp.where(lax.rem(j, 2) == 1, z - d, z + d)
        far = jnp.where(z < Z - 1 - z, j, Z - 1 - j)
        return jnp.where(j <= 2 * low, near, far)

    def along(zc, way):
        block = gath.at[2 * zc + g]
        return remote(block, block, ga_send.at[way, zc], ga_recv.at[zc], sp, tp + 2 - 4 * way)

    def across(zc):
        block = gath.at[2 * zc + g]
        return remote(block, block, d2_send.at[zc], d2_recv.at[zc], sp, partner)

    ring = outg.shape[0]

    def dispatch(j, ds):
        zc = chip_at(j)
        to = lax.rem(sp + ds, S)
        return remote(outg.at[lax.rem(j, ring), to], arr.at[zc, sp], dis_send.at[zc, ds - 1],
                      dis_recv.at[zc, ds - 1], to, tp)

    def give_back(zc, ds):
        to = lax.rem(sp + ds, S)
        return remote(arr.at[zc, to], back.at[zc, sp], ret_send.at[zc, ds - 1],
                      ret_recv.at[zc, ds - 1], to, tp)

    def merge(zc):
        return remote(gath.at[2 * zc + 1 - g], prem.at[zc], pd_send.at[zc], pd_recv.at[zc],
                      sp, partner)

    def deliver(zc):
        return remote(gath.at[2 * zc + g], zrec.at[z], zs_send.at[zc], zs_recv.at[z],
                      sp, 2 * zc + g)

    def gather_step(j):
        zc = chip_at(j)

        @pl.when(j > 0)
        def _():
            pltpu.make_async_copy(gath.at[2 * zc + g], gath.at[2 * zc + g], ga_recv.at[zc]).wait()

        across(zc).start()

        @pl.when((zc <= z) & (z < Z - 1))
        def _():
            along(zc, 0).start()

        @pl.when((zc >= z) & (z > 0))
        def _():
            along(zc, 1).start()

        @pl.when(j == min(1, Z - 1))
        def _():
            for d in range(1, L):
                weight_copy(2, d).start()

        across(zc).wait_recv()
        slot_id = lax.broadcasted_iota(jnp.int32, (slots, 2 * rows), 0)
        hit = slot_id == sel_ref[zc, 0:1, :]
        for k in range(1, sel_ref.shape[1]):
            hit = hit | (slot_id == sel_ref[zc, k : k + 1, :])
        selector = jnp.where(hit, 1.0, 0.0).astype(jnp.bfloat16)
        slot = lax.rem(j, ring)

        @pl.when(j >= ring)
        def _():
            for ds in range(1, S):
                dispatch(j - ring, ds).wait_send()

        def pick(n, _):
            cols = pl.ds(pl.multiple_of(n * wide, wide), wide)
            tokens = gath[pl.ds(2 * zc, 2), :, cols].reshape(2 * rows, wide)
            picked = jnp.dot(selector, tokens, preferred_element_type=jnp.float32)
            outg[slot, :, :, cols] = picked.astype(jnp.bfloat16).reshape(S, two_cap, wide)
            return 0

        lax.fori_loop(0, D // wide, pick, 0)
        for ds in range(1, S):
            dispatch(j, ds).start()
        arr[zc, sp] = outg[slot, sp]

    def expert_step(j):
        zc = chip_at(j)

        @pl.when(j == 0)
        def _():
            for c in own_weights:
                c.wait()
            for i in range(3):
                for d in range(1, L):
                    weight_copy(i, d).wait_recv()

        for ds in range(1, S):
            dispatch(j, ds).wait_recv()

        def activate(x, gate_w, up_w):
            gate_act = jnp.dot(x, gate_w, preferred_element_type=jnp.float32)
            up_act = jnp.dot(x, up_w, preferred_element_type=jnp.float32)
            return (jax.nn.silu(gate_act) * up_act).astype(jnp.bfloat16)

        x = arr[zc].reshape(slots, D)
        if len(wg.shape) == 3:
            for n in range(L):
                hid[:, n * F : (n + 1) * F] = activate(x, wg[n], wu[n])
        else:
            span = min(256, L * F)

            def up(n, _):
                cols = pl.ds(pl.multiple_of(n * span, span), span)
                hid[:, cols] = activate(arr[zc].reshape(slots, D), wg[:, cols], wu[:, cols])
                return 0

            if span == L * F:
                hid[...] = activate(x, wg[...], wu[...])
            else:
                lax.fori_loop(0, L * F // span, up, 0)

        def down(n, _):
            cols = pl.ds(pl.multiple_of(n * wide, wide), wide)
            rows_out = jnp.dot(hid[...], wd[:, cols], preferred_element_type=jnp.float32)
            arr[zc, :, :, cols] = rows_out.astype(jnp.bfloat16).reshape(S, two_cap, wide)
            return 0

        lax.fori_loop(0, D // wide, down, 0)

        @pl.when(j > 0)
        def _():
            for ds in range(1, S):
                give_back(zc, ds).start()

    def stage(j, _):
        @pl.when(j < Z)
        def _():
            gather_step(j)

        @pl.when(j >= LAG)
        def _():
            expert_step(j - LAG)

        return 0

    lax.fori_loop(0, Z + LAG, stage, 0)
    for ds in range(1, S):
        give_back(z, ds).start()

    def combine(i, _):
        zc = chip_at(lax.rem(i + 1, Z))
        across(zc).wait_send()

        @pl.when((zc <= z) & (z < Z - 1))
        def _():
            along(zc, 0).wait_send()

        @pl.when((zc >= z) & (z > 0))
        def _():
            along(zc, 1).wait_send()

        for ds in range(1, S):
            give_back(zc, ds).wait_recv()
        back[zc, sp] = arr[zc, sp]
        slot_id = lax.broadcasted_iota(jnp.int32, (2 * rows, slots), 1)
        table = jnp.zeros((2 * rows, slots), jnp.float32)
        for k in range(comb_ref.shape[2]):
            table = jnp.where(
                slot_id == comb_ref[zc, :, k : k + 1], wt_ref[zc, :, k : k + 1], table
            )
        high, low = split_f32(table)

        def mix(n, _):
            cols = pl.ds(pl.multiple_of(n * wide, wide), wide)
            values = back[zc, :, :, cols].reshape(slots, wide)
            total = jnp.dot(high, values, preferred_element_type=jnp.float32)
            total = total + jnp.dot(low, values, preferred_element_type=jnp.float32)
            pbuf[:, :, cols] = total.reshape(2, rows, wide)
            return 0

        lax.fori_loop(0, D // wide, mix, 0)
        gath[2 * zc + 1 - g] = pbuf[1 - g].astype(jnp.bfloat16)
        merge(zc).start()
        merge(zc).wait_recv()

        @pl.when(zc != z)
        def _():
            gath[2 * zc + g] = (pbuf[g] + prem[zc].astype(jnp.float32)).astype(jnp.bfloat16)
            deliver(zc).start()

        return 0

    lax.fori_loop(0, Z, combine, 0)

    def arrived(zc):
        return pltpu.make_async_copy(zrec.at[zc], zrec.at[zc], zs_recv.at[zc])

    for d in range(1, Z):
        arrived(lax.rem(z + d, Z)).wait()

    def finish(n, _):
        at = pl.ds(pl.multiple_of(n * part, part), part)
        total = pbuf[g, at, :] + prem[z, at, :].astype(jnp.float32)
        for d in range(1, Z):
            total = total + zrec[lax.rem(z + d, Z), at, :].astype(jnp.float32)
        mixture = total.astype(jnp.bfloat16)
        out_ref[at, :] = (
            stream[at, :].astype(jnp.float32) + norm_rows(mixture, gain_ref[2:3, :])
        ).astype(jnp.bfloat16)
        return 0

    lax.fori_loop(0, rows // part, finish, 0)
    for i in range(3):
        for d in range(1, L):
            weight_copy(i, d).wait_send()
    for j in range(max(0, Z - ring), Z):
        for ds in range(1, S):
            dispatch(j, ds).wait_send()
    for zc in range(Z):
        for ds in range(1, S):
            give_back(zc, ds).wait_send()
        merge(zc).wait_send()
    for d in range(1, Z):
        deliver(lax.rem(z + d, Z)).wait_send()


def on_device(
    mix_in, gate_in, conv_w, conv_b, decay_param, recur_gate, recur_bias, input_gate, input_bias,
    residual, out_proj, norm_gain, routes, route_wt, exp_gate, exp_up, exp_down,
):
    S, T = lax.axis_size("sp"), lax.axis_size("tp")
    L, D, F = exp_gate.shape
    Z = T // 2
    dims = (S, T, L, Z)
    seq, C = mix_in.shape
    rows = residual.shape[0]
    cap = 2 * rows * routes.shape[1] // (L * S)
    local = lax.rem(lax.axis_index("tp"), L)
    sel, comb, weights = slot_tables(routes, route_wt, dims, rows, cap, local)
    soft = jax.nn.softplus(-decay_param)
    vmem = pl.BlockSpec(memory_space=pltpu.VMEM)
    hbm = pl.BlockSpec(memory_space=pltpu.MemorySpace.HBM)
    b16, f32 = jnp.bfloat16, jnp.float32
    dma = pltpu.SemaphoreType.DMA
    up_shape = (D, L * F) if F % 128 == 0 or L == 1 else (L, D, F)
    return pl.pallas_call(
        functools.partial(layer_kernel, dims),
        out_shape=jax.ShapeDtypeStruct((rows, D), b16),
        in_specs=[vmem] * 14 + [hbm] * 4,
        out_specs=vmem,
        scratch_shapes=[
            pltpu.VMEM((seq + 2 * SUB, C), f32),
            pltpu.VMEM((C, 4 * C), b16),
            pltpu.VMEM((C, 4 * C), b16),
            pltpu.VMEM((seq, C), f32), pltpu.VMEM((seq, C), f32),
            pltpu.VMEM((seq, C), f32), pltpu.VMEM((seq, C), f32),
            pltpu.VMEM((seq, C), b16),
            pltpu.VMEM((rows, T * C), b16),
            pltpu.VMEM(out_proj.shape, b16),
            pltpu.VMEM((rows, D), b16),
            pltpu.VMEM((2, HALO, C), b16),
            pltpu.VMEM((SUB, C), f32),
            pltpu.VMEM((S - 1, SUB, C), f32),
            pltpu.VMEM(up_shape, b16), pltpu.VMEM(up_shape, b16), pltpu.VMEM((L * F, D), b16),
            pltpu.VMEM((S * 2 * cap, L * F), b16),
            pltpu.VMEM((rows, D), b16),
            pltpu.VMEM((T, rows, D), b16),
            pltpu.VMEM((min(Z, RING), S, 2 * cap, D), b16),
            pltpu.VMEM((Z, S, 2 * cap, D), b16),
            pltpu.VMEM((Z, S, 2 * cap, D), b16),
            pltpu.VMEM((Z, rows, D), b16),
            pltpu.VMEM((Z, rows, D), b16),
            pltpu.VMEM((2, rows, D), f32),
            dma, dma((8,)),
            dma((2,)), dma((2,)),
            dma((S - 1,)), dma((S - 1,)),
            dma((T,)), dma((T,)),
            dma((max(L - 1, 1), 3)), dma((max(L - 1, 1), 3)),
            dma((2, Z)), dma((Z,)),
            dma((Z,)), dma((Z,)),
            dma((Z, S - 1)), dma((Z, S - 1)),
            dma((Z, S - 1)), dma((Z, S - 1)),
            dma((Z,)), dma((Z,)),
            dma((Z,)), dma((Z,)),
        ],
        compiler_params=pltpu.CompilerParams(
            collective_id=0, has_side_effects=True, vmem_limit_bytes=62 * 1024 * 1024
        ),
    )(
        mix_in, gate_in, conv_w, conv_b.reshape(1, C), soft, recur_gate, recur_bias, input_gate,
        input_bias, residual, norm_gain, sel, comb, weights, out_proj, exp_gate, exp_up, exp_down,
    )


def solution(mesh):
    return jax.shard_map(
        on_device,
        mesh=mesh,
        in_specs=(
            P("sp", "tp"),
            P("sp", "tp"),
            P(None, "tp"),
            P("tp"),
            P(None, "tp"),
            P(None, "tp", None, None),
            P(None, "tp"),
            P(None, "tp", None, None),
            P(None, "tp"),
            P(("sp", "tp"), None),
            P(),
            P(),
            P("sp", None),
            P("sp", None),
            P("sp", None, "tp"),
            P("sp", None, "tp"),
            P("sp", "tp", None),
        ),
        out_specs=P(("sp", "tp"), None),
        check_vma=False,
    )
```

time: 277 us -> 207 us (0.75)
  Pallas kernels: 251 us -> 199 us
  matrix products: 19.5 us -> 0.2 us
  local copies, waits for them, and re-layouts: 1.94 us -> 5.97 us
    pallas_call x2 -> x1, Pallas kernels: 251 us -> 199 us  [on_device(): pl.pallas_call(functools.partial(layer_kernel, dims), out_shape=jax.Shape...]
    dot_general x4 -> x1, matrix products: 19.5 us -> 0.2 us  [slot_tables(): jnp.dot(before, matches.reshape(rows * top, T * S).astype(jnp.bfloat16),...]
    unnamed x8 -> x7, local copies, waits for them, and re-layouts: 0.02 us -> 3.83 us
where the time goes in v1:
time: 207 us
  Pallas kernels  199 us (96%)
  local copies, waits for them, and re-layouts  5.97 us (3%)
    pallas_call x1, Pallas kernels, on_device(): pl.pallas_call(functools.partial(layer_kernel, dims), out_shape=jax.Shape...  199 us

profile of v1, /device:TPU:0, one launch (start us, length us, event | category | flops | bytes accessed | tf_op | source)
XLA Modules:
  0.0 206.6 jit_solution(5353021867061739909)
XLA Ops:
  0.0 0.0 copy-start.1
  0.0 0.1 add_multiply_fusion
  0.1 1.3 compare_select_fusion.soft_ref
  1.4 0.1 eq.31
  1.5 0.9 copy.26
  2.4 0.3 reshape.69
  2.7 0.1 compare_bitcast_fusion
  2.8 0.2 fusion.3
  3.0 0.1 copy.29
  3.1 0.8 copy.30
  4.0 0.0 copy-start
  4.0 0.8 copy.32.sel_ref
  4.8 0.0 copy-done.1
  4.8 1.0 copy.31
  5.8 0.0 copy-done
  5.8 198.9 %shard_map.163 = bf16[128,2048]{1,0:T(8,128)(2,1)} custom-call(bf16[1024,256]{1,0:T(8,128)(2,1)} %mix_ref.1, bf16[1024,256]{1,0:T(8,128)(2,1)} %gate_ref.1, f32[4,256]{1,0:T(4,128)} %cw_ref.1, f32[1,256]{1,0:T(1,128)} %bitcast.22, f32[2,256]{1,0:T(2,128)} %compare_select_fusion.soft_ref, f32[2,4,64,64]{3,2,1,0:T(8,128)} %rg_ref.1, f32[2,256]{1,0:T(2,128)} %rb_ref.1, ...), custom_call_target="tpu_custom_call" | custom-call | tf_op jit(solution)/shard_map/pallas_call | solution.py:529
  204.7 1.9 copy.37
  (8 shorter events, 0.1 us)
Async XLA Ops:
  0.0 4.8 %copy-start.1 = (f32[1024,2]{0,1:T(2,128)S(1)}, f32[1024,2]{0,1:T(2,128)}, u32[]{:S(2)}) copy-start(f32[1024,2]{0,1:T(2,128)} %param.30) | copy-start | bytes 24580
  4.0 1.8 copy-start

commit v2 on v1

--- a/solution.py
+++ b/solution.py
@@ -12,35 +12,12 @@
 MESH = pl.DeviceIdType.MESH
 HALO = 16
 SUB = 8
-LAG = 2
 RING = 2
 
 
 def norm_rows(values, gain):
     floats = values.astype(jnp.float32)
     return floats * lax.rsqrt(jnp.mean(floats * floats, axis=-1, keepdims=True) + EPSILON) * gain
-
-
-def slot_tables(routes, route_wt, dims, rows, cap, local):
-    S, T, L, Z = dims
-    top = routes.shape[1]
-    pair = 2 * rows
-    flat = routes.reshape(T, rows * top).T
-    wanted = jnp.arange(S, dtype=jnp.int32) * L + local
-    matches = flat[:, :, None] == wanted
-    order = jnp.arange(rows * top, dtype=jnp.int32)
-    before = (order[None, :] < order[:, None]).astype(jnp.bfloat16)
-    earlier = jnp.dot(
-        before, matches.reshape(rows * top, T * S).astype(jnp.bfloat16),
-        preferred_element_type=jnp.float32,
-    ).reshape(rows * top, T, S)
-    core = (jnp.arange(T, dtype=jnp.int32) % 2)[:, None]
-    slot = (jnp.arange(S, dtype=jnp.int32) * 2 + core) * cap
-    ids = jnp.where(matches, earlier.astype(jnp.int32) + slot + 1, 0).sum(axis=2) - 1
-    ids = ids.reshape(rows, top, T)
-    by_slot = ids.transpose(2, 0, 1).reshape(Z, pair, top)
-    weights = route_wt.reshape(Z, pair, top)
-    return by_slot.transpose(0, 2, 1), by_slot, weights
 
 
 def one_minus_exp(y):
@@ -69,14 +46,15 @@
 
 def layer_kernel(
     dims,
-    mix_ref, gate_ref, cw_ref, cb_ref, soft_ref, rg_ref, rb_ref, ig_ref, ib_ref,
-    res_ref, gain_ref, sel_ref, comb_ref, wt_ref, op_hbm, eg_hbm, eu_hbm, ed_hbm,
-    out_ref,
+    mix_ref, gate_ref, cw_ref, cb_ref, decay_ref, rg_ref, rb_ref, ig_ref, ib_ref,
+    res_ref, gain_ref, routes_ref, wt_ref, op_hbm, eg_hbm, eu_hbm, ed_hbm,
+    stream, delta_ref,
     xp, wh, wl, af, bf, ab, bb, mixed, tok, op, proj, halo, summ, ends,
-    wg, wu, wd, hid, stream, gath, outg, arr, back, prem, zrec, pbuf,
+    soft_ref, wg, wu, wd, hid, gath, outg, arr, back, prem, zrec, pin, pbuf,
     op_sem, own_sem, halo_send, halo_recv, sum_send, sum_recv,
-    mix_send, mix_recv, w_send, w_recv, ga_send, ga_recv, d2_send, d2_recv,
+    mix_send, mix_recv, w_send, w_recv, p_send, p_recv, ga_send, ga_recv, d2_send, d2_recv,
     dis_send, dis_recv, ret_send, ret_recv, pd_send, pd_recv, zs_send, zs_recv,
+    pin_send, pin_recv,
 ):
     S, T, L, Z = dims
     seq, C = mix_ref.shape
@@ -89,8 +67,13 @@
     tp = lax.axis_index("tp")
     z = lax.div(tp, 2)
     g = lax.rem(tp, 2)
-    local = lax.rem(tp, L)
-    part_base = tp - local
+    local = 2 * (1 - lax.rem(z, 2)) + g if L > 1 else 0
+    upward = z < Z // 2
+    inward = jnp.where(upward, z + 1, z - 1)
+    middle = (z > 0) & (z < Z - 1) & (L > 1)
+    cap = two_cap // 2
+    top = routes_ref.shape[0]
+    pair_width = 2 * F if L > 1 else F
     partner = tp + 1 - 2 * g
 
     op_copy = pltpu.make_async_copy(op_hbm, op, op_sem)
@@ -107,7 +90,6 @@
                     device_id_type=MESH,
                 )
                 greeted += 1
-    pl.semaphore_wait(barrier, greeted)
 
     def remote(src, dst, send, recv, sp_to, tp_to):
         return pltpu.make_async_remote_copy(
@@ -119,34 +101,58 @@
                      halo_recv.at[0], lax.rem(sp + 1, S), tp)
     to_prev = remote(mix_ref.at[pl.ds(0, HALO)], halo.at[1], halo_send.at[1],
                      halo_recv.at[1], lax.rem(sp + S - 1, S), tp)
-    to_next.start()
-    to_prev.start()
 
     tensors = ((eg_hbm, wg, 1), (eu_hbm, wu, 1), (ed_hbm, wd, 0))
+    depth = eg_hbm.shape[1]
+    pieces = (
+        (eg_hbm, wg, 1, 0, depth), (eu_hbm, wu, 1, 0, depth // 2),
+        (eu_hbm, wu, 1, depth // 2, depth // 2), (ed_hbm, wd, 0, 0, F),
+    )
 
     def chunk(ref, axis, place):
-        if len(ref.shape) == 3:
-            return ref.at[place]
         if ref.shape[axis] == F:
             return ref
         start = pl.multiple_of(place * F, F)
         return ref.at[:, pl.ds(start, F)] if axis else ref.at[pl.ds(start, F), :]
 
-    def weight_copy(i, d):
+    def weight_copy(i, core):
+        src, dst, axis, first, count = pieces[i]
+        side = jnp.where(upward, 0, 1)
+        at = pl.ds(first, count)
+        return remote(src.at[2 * lax.rem(z, 2) + core].at[at],
+                      chunk(dst, axis, 2 + 2 * side + g).at[at],
+                      w_send.at[i, core], w_recv.at[i, 2 * side + g], sp, 2 * inward + core)
+
+    def partner_copy(i):
         src, dst, axis = tensors[i]
-        to = lax.rem(local + d, L)
-        return remote(src.at[to], chunk(dst, axis, local), w_send.at[d - 1, i],
-                      w_recv.at[d - 1, i], sp, part_base + to)
+        return remote(src.at[local + 1 - 2 * g], chunk(dst, axis, g), p_send.at[i],
+                      p_recv.at[i], sp, partner)
 
     own_weights = [
-        pltpu.make_async_copy(src.at[local], chunk(dst, axis, local), own_sem.at[i])
+        pltpu.make_async_copy(src.at[local], chunk(dst, axis, g if L > 1 else 0), own_sem.at[i])
         for i, (src, dst, axis) in enumerate(tensors)
     ]
+
+    def start_weights(core, which):
+        if L > 1:
+            for i in which:
+                weight_copy(i, core).start()
+
+    def chip_weights_arrived():
+        for i in range(3):
+            own_weights[i].wait()
+            if L > 1:
+                partner_copy(i).wait_recv()
+
+    def weights_arrived(which):
+        for i in which:
+            for k in range(4):
+                _, dst, axis, first, count = pieces[i]
+                block = chunk(dst, axis, 2 + k).at[pl.ds(first, count)]
+                pltpu.make_async_copy(block, block, w_recv.at[i, k]).wait()
+
     for c in own_weights:
         c.start()
-    for i in range(2):
-        for d in range(1, L):
-            weight_copy(i, d).start()
 
     wh[...] = jnp.zeros_like(wh)
     wl[...] = jnp.zeros_like(wl)
@@ -158,12 +164,14 @@
                 wh[h * hd : (h + 1) * hd, col : col + hd] = high
                 wl[h * hd : (h + 1) * hd, col : col + hd] = low
     xp[SUB : SUB + seq, :] = mix_ref[...].astype(jnp.float32)
-    to_next.wait()
-    to_prev.wait()
-    tail = halo[0].astype(jnp.float32)[HALO - SUB : HALO]
-    head = halo[1].astype(jnp.float32)[0:SUB]
-    xp[0:SUB, :] = jnp.where(sp > 0, tail, 0.0)
-    xp[SUB + seq : 2 * SUB + seq, :] = jnp.where(sp < S - 1, head, 0.0)
+    soft_ref[...] = jax.nn.softplus(-decay_ref[...])
+    pl.semaphore_wait(barrier, greeted)
+    to_next.start()
+    to_prev.start()
+    start_weights(0, (0, 1))
+    if L > 1:
+        for i in range(3):
+            partner_copy(i).start()
 
     R = min(128, seq)
 
@@ -191,7 +199,14 @@
             b_ref[pl.ds(base, R), :] = b.reshape(R, C)
         return 0
 
-    lax.fori_loop(0, seq // R, gates, 0)
+    lax.fori_loop(1, seq // R - 1, gates, 0)
+    to_next.wait()
+    to_prev.wait()
+    tail = halo[0].astype(jnp.float32)[HALO - SUB : HALO]
+    head = halo[1].astype(jnp.float32)[0:SUB]
+    xp[0:SUB, :] = jnp.where(sp > 0, tail, 0.0)
+    xp[SUB + seq : 2 * SUB + seq, :] = jnp.where(sp < S - 1, head, 0.0)
+    lax.fori_loop(0, 2, lambda n, _: gates(n * (seq // R - 1), 0), 0)
 
     tiles = seq // SUB
 
@@ -255,6 +270,7 @@
         c.start()
     own_move = pltpu.make_async_copy(block_rows(tp), tok.at[:, columns], own_sem.at[6])
     own_move.start()
+    start_weights(0, (2,))
     op_copy.wait()
     own_move.wait()
     for c in moves:
@@ -319,6 +335,34 @@
         return remote(gath.at[2 * zc + g], zrec.at[z], zs_send.at[zc], zs_recv.at[z],
                       sp, 2 * zc + g)
 
+    def slot_table(zc, weighted):
+        at = pl.ds(pl.multiple_of(zc * (2 * rows), 2 * rows), 2 * rows)
+        named, given = routes_ref[:, at], wt_ref[:, at]
+        high_rows = max(16, S)
+        experts = lax.broadcasted_iota(jnp.int32, (high_rows, 2 * rows), 0) * L + local
+        hit = experts == named[0:1]
+        share = jnp.where(hit, given[0:1], 0.0)
+        for k in range(1, top):
+            same = experts == named[k : k + 1]
+            hit = hit | same
+            share = jnp.where(same, given[k : k + 1], share)
+        earlier = lax.broadcasted_iota(jnp.int32, (2 * rows, 2 * rows), 0)
+        token = lax.broadcasted_iota(jnp.int32, (2 * rows, 2 * rows), 1)
+        inside = jnp.where(token >= rows, rows, 0)
+        before = jnp.where((earlier < token) & (earlier >= inside), 1.0, 0.0)
+        rank = jnp.dot(
+            jnp.where(hit, 1.0, 0.0).astype(jnp.bfloat16), before.astype(jnp.bfloat16),
+            preferred_element_type=jnp.float32,
+        ).astype(jnp.int32)
+        column = lax.broadcasted_iota(jnp.int32, (high_rows, 2 * rows), 1)
+        place = jnp.where(hit, rank + jnp.where(column >= rows, cap, 0), -1)
+        slot_id = lax.broadcasted_iota(jnp.int32, (two_cap, 2 * rows), 0)
+        pieces = [
+            jnp.where(slot_id == place[s : s + 1], share[s : s + 1] if weighted else 1.0, 0.0)
+            for s in range(S)
+        ]
+        return jnp.concatenate(pieces, axis=0)
+
     def gather_step(j):
         zc = chip_at(j)
 
@@ -336,17 +380,13 @@
         def _():
             along(zc, 1).start()
 
-        @pl.when(j == min(1, Z - 1))
-        def _():
-            for d in range(1, L):
-                weight_copy(2, d).start()
+        @pl.when(zc == jnp.where(upward, 0, Z - 1))
+        def _():
+            start_weights(0, (3,))
+            start_weights(1, (0, 1, 2, 3))
 
         across(zc).wait_recv()
-        slot_id = lax.broadcasted_iota(jnp.int32, (slots, 2 * rows), 0)
-        hit = slot_id == sel_ref[zc, 0:1, :]
-        for k in range(1, sel_ref.shape[1]):
-            hit = hit | (slot_id == sel_ref[zc, k : k + 1, :])
-        selector = jnp.where(hit, 1.0, 0.0).astype(jnp.bfloat16)
+        selector = slot_table(zc, False).astype(jnp.bfloat16)
         slot = lax.rem(j, ring)
 
         @pl.when(j >= ring)
@@ -366,72 +406,118 @@
             dispatch(j, ds).start()
         arr[zc, sp] = outg[slot, sp]
 
-    def expert_step(j):
+    def activate(x, gate_w, up_w):
+        gate_act = jnp.dot(x, gate_w, preferred_element_type=jnp.float32)
+        up_act = jnp.dot(x, up_w, preferred_element_type=jnp.float32)
+        return (jax.nn.silu(gate_act) * up_act).astype(jnp.bfloat16)
+
+    def up_part(j, n):
         zc = chip_at(j)
-
-        @pl.when(j == 0)
-        def _():
-            for c in own_weights:
-                c.wait()
-            for i in range(3):
-                for d in range(1, L):
-                    weight_copy(i, d).wait_recv()
-
-        for ds in range(1, S):
-            dispatch(j, ds).wait_recv()
-
-        def activate(x, gate_w, up_w):
-            gate_act = jnp.dot(x, gate_w, preferred_element_type=jnp.float32)
-            up_act = jnp.dot(x, up_w, preferred_element_type=jnp.float32)
-            return (jax.nn.silu(gate_act) * up_act).astype(jnp.bfloat16)
-
-        x = arr[zc].reshape(slots, D)
-        if len(wg.shape) == 3:
-            for n in range(L):
-                hid[:, n * F : (n + 1) * F] = activate(x, wg[n], wu[n])
-        else:
-            span = min(256, L * F)
-
-            def up(n, _):
-                cols = pl.ds(pl.multiple_of(n * span, span), span)
-                hid[:, cols] = activate(arr[zc].reshape(slots, D), wg[:, cols], wu[:, cols])
-                return 0
-
-            if span == L * F:
-                hid[...] = activate(x, wg[...], wu[...])
-            else:
-                lax.fori_loop(0, L * F // span, up, 0)
+        cols = pl.ds(pl.multiple_of(n * pair_width, pair_width), pair_width)
+        if L == 1:
+            cols = slice(None)
+        hid[j, :, cols] = activate(arr[zc].reshape(slots, D), wg[:, cols], wu[:, cols])
+
+    def down_part(j, depth):
+        zc = chip_at(j)
 
         def down(n, _):
             cols = pl.ds(pl.multiple_of(n * wide, wide), wide)
-            rows_out = jnp.dot(hid[...], wd[:, cols], preferred_element_type=jnp.float32)
+            rows_out = jnp.dot(
+                hid[j, :, :depth], wd[:depth, cols], preferred_element_type=jnp.float32
+            )
             arr[zc, :, :, cols] = rows_out.astype(jnp.bfloat16).reshape(S, two_cap, wide)
             return 0
 
         lax.fori_loop(0, D // wide, down, 0)
 
-        @pl.when(j > 0)
-        def _():
-            for ds in range(1, S):
-                give_back(zc, ds).start()
+    def return_rows(zc):
+        for ds in range(1, S):
+            give_back(zc, ds).start()
+
+    early = middle & (g == 0)
 
     def stage(j, _):
         @pl.when(j < Z)
         def _():
             gather_step(j)
 
-        @pl.when(j >= LAG)
-        def _():
-            expert_step(j - LAG)
+        @pl.when(j == 1)
+        def _():
+            chip_weights_arrived()
+            if L > 1:
+
+                @pl.when(early)
+                def _():
+                    weights_arrived((0, 1, 2))
+
+        @pl.when(j > 0)
+        def _():
+            for ds in range(1, S):
+                dispatch(j - 1, ds).wait_recv()
+
+            def part_of(n, _):
+                up_part(j - 1, n)
+                return 0
+
+            lax.fori_loop(0, jnp.where(early, 3, 1), part_of, 0)
+
+            @pl.when(jnp.logical_not(middle))
+            def _():
+                down_part(j - 1, pair_width)
+
+                @pl.when(j > 1)
+                def _():
+                    return_rows(chip_at(j - 1))
 
         return 0
 
-    lax.fori_loop(0, Z + LAG, stage, 0)
-    for ds in range(1, S):
-        give_back(z, ds).start()
+    lax.fori_loop(0, Z + 1, stage, 0)
+
+    @pl.when(jnp.logical_not(middle))
+    def _():
+        return_rows(z)
+
+    if L > 1:
+
+        @pl.when(middle)
+        def _():
+            @pl.when(g == 1)
+            def _():
+                weights_arrived((0, 1, 2))
+
+                def rest(n, _):
+                    up_part(lax.div(n, 2), 1 + lax.rem(n, 2))
+                    return 0
+
+                lax.fori_loop(0, 2 * Z, rest, 0)
+
+            weights_arrived((3,))
+
+            def finish_rows(i, _):
+                down_part(Z - 1 - i, 3 * pair_width)
+                return_rows(chip_at(Z - 1 - i))
+                return 0
+
+            lax.fori_loop(0, Z, finish_rows, 0)
+
+    pair_chip = z + 1 - 2 * lax.rem(z, 2)
+
+    def return_order(i):
+        return chip_at(jnp.where(middle, Z - 1 - i, lax.rem(i + 1, Z)))
+
+    def feeds(zc):
+        return (zc != z) & (zc != pair_chip) & ((zc > z) == (lax.rem(z, 2) == 0))
+
+    def relays(zc):
+        return (zc != z) & (zc != pair_chip) & ((zc > z) != (lax.rem(z, 2) == 0))
+
+    def feed(zc):
+        return remote(gath.at[2 * zc + g], pin.at[zc], pin_send.at[zc], pin_recv.at[zc],
+                      sp, 2 * pair_chip + g)
 
     def combine(i, _):
-        zc = chip_at(lax.rem(i + 1, Z))
+        zc = return_order(i)
         across(zc).wait_send()
 
         @pl.when((zc <= z) & (z < Z - 1))
@@ -445,12 +531,7 @@
         for ds in range(1, S):
             give_back(zc, ds).wait_recv()
         back[zc, sp] = arr[zc, sp]
-        slot_id = lax.broadcasted_iota(jnp.int32, (2 * rows, slots), 1)
-        table = jnp.zeros((2 * rows, slots), jnp.float32)
-        for k in range(comb_ref.shape[2]):
-            table = jnp.where(
-                slot_id == comb_ref[zc, :, k : k + 1], wt_ref[zc, :, k : k + 1], table
-            )
+        table = jnp.transpose(slot_table(zc, True))
         high, low = split_f32(table)
 
         def mix(n, _):
@@ -466,9 +547,24 @@
         merge(zc).start()
         merge(zc).wait_recv()
 
-        @pl.when(zc != z)
+        @pl.when(feeds(zc) | (zc == pair_chip))
         def _():
             gath[2 * zc + g] = (pbuf[g] + prem[zc].astype(jnp.float32)).astype(jnp.bfloat16)
+
+        @pl.when(feeds(zc))
+        def _():
+            feed(zc).start()
+
+        @pl.when(relays(zc))
+        def _():
+            pltpu.make_async_copy(pin.at[zc], pin.at[zc], pin_recv.at[zc]).wait()
+            gath[2 * zc + g] = (
+                pbuf[g] + prem[zc].astype(jnp.float32) + pin[zc].astype(jnp.float32)
+            ).astype(jnp.bfloat16)
+            deliver(zc).start()
+
+        @pl.when(zc == pair_chip)
+        def _():
             deliver(zc).start()
 
         return 0
@@ -478,24 +574,29 @@
     def arrived(zc):
         return pltpu.make_async_copy(zrec.at[zc], zrec.at[zc], zs_recv.at[zc])
 
-    for d in range(1, Z):
-        arrived(lax.rem(z + d, Z)).wait()
+    senders = [pair_chip]
+    for m in range(1, Z // 2):
+        other = lax.rem(lax.div(z, 2) + m, Z // 2)
+        senders.append(2 * other + jnp.where(2 * other < z, 1, 0))
+    for zc in senders:
+        arrived(zc).wait()
 
     def finish(n, _):
         at = pl.ds(pl.multiple_of(n * part, part), part)
         total = pbuf[g, at, :] + prem[z, at, :].astype(jnp.float32)
-        for d in range(1, Z):
-            total = total + zrec[lax.rem(z + d, Z), at, :].astype(jnp.float32)
+        for zc in senders:
+            total = total + zrec[zc, at, :].astype(jnp.float32)
         mixture = total.astype(jnp.bfloat16)
-        out_ref[at, :] = (
-            stream[at, :].astype(jnp.float32) + norm_rows(mixture, gain_ref[2:3, :])
-        ).astype(jnp.bfloat16)
+        delta_ref[at, :] = norm_rows(mixture, gain_ref[2:3, :])
         return 0
 
     lax.fori_loop(0, rows // part, finish, 0)
-    for i in range(3):
-        for d in range(1, L):
-            weight_copy(i, d).wait_send()
+    if L > 1:
+        for i in range(3):
+            partner_copy(i).wait_send()
+        for i in range(4):
+            for core in range(2):
+                weight_copy(i, core).wait_send()
     for j in range(max(0, Z - ring), Z):
         for ds in range(1, S):
             dispatch(j, ds).wait_send()
@@ -503,8 +604,21 @@
         for ds in range(1, S):
             give_back(zc, ds).wait_send()
         merge(zc).wait_send()
-    for d in range(1, Z):
-        deliver(lax.rem(z + d, Z)).wait_send()
+
+    def drain(i, _):
+        zc = return_order(i)
+
+        @pl.when(feeds(zc))
+        def _():
+            feed(zc).wait_send()
+
+        @pl.when((zc != z) & jnp.logical_not(feeds(zc)))
+        def _():
+            deliver(zc).wait_send()
+
+        return 0
+
+    lax.fori_loop(0, Z, drain, 0)
 
 
 def on_device(
@@ -518,19 +632,17 @@
     seq, C = mix_in.shape
     rows = residual.shape[0]
     cap = 2 * rows * routes.shape[1] // (L * S)
-    local = lax.rem(lax.axis_index("tp"), L)
-    sel, comb, weights = slot_tables(routes, route_wt, dims, rows, cap, local)
-    soft = jax.nn.softplus(-decay_param)
     vmem = pl.BlockSpec(memory_space=pltpu.VMEM)
     hbm = pl.BlockSpec(memory_space=pltpu.MemorySpace.HBM)
     b16, f32 = jnp.bfloat16, jnp.float32
     dma = pltpu.SemaphoreType.DMA
-    up_shape = (D, L * F) if F % 128 == 0 or L == 1 else (L, D, F)
-    return pl.pallas_call(
+    hidden = 6 * F if L > 1 else F
+    up_shape = (D, hidden)
+    stream, delta = pl.pallas_call(
         functools.partial(layer_kernel, dims),
-        out_shape=jax.ShapeDtypeStruct((rows, D), b16),
-        in_specs=[vmem] * 14 + [hbm] * 4,
-        out_specs=vmem,
+        out_shape=(jax.ShapeDtypeStruct((rows, D), b16), jax.ShapeDtypeStruct((rows, D), f32)),
+        in_specs=[vmem] * 13 + [hbm] * 4,
+        out_specs=(vmem, vmem),
         scratch_shapes=[
             pltpu.VMEM((seq + 2 * SUB, C), f32),
             pltpu.VMEM((C, 4 * C), b16),
@@ -544,13 +656,14 @@
             pltpu.VMEM((2, HALO, C), b16),
             pltpu.VMEM((SUB, C), f32),
             pltpu.VMEM((S - 1, SUB, C), f32),
-            pltpu.VMEM(up_shape, b16), pltpu.VMEM(up_shape, b16), pltpu.VMEM((L * F, D), b16),
-            pltpu.VMEM((S * 2 * cap, L * F), b16),
-            pltpu.VMEM((rows, D), b16),
+            pltpu.VMEM((2, C), f32),
+            pltpu.VMEM(up_shape, b16), pltpu.VMEM(up_shape, b16), pltpu.VMEM((hidden, D), b16),
+            pltpu.VMEM((Z, S * 2 * cap, hidden), b16),
             pltpu.VMEM((T, rows, D), b16),
             pltpu.VMEM((min(Z, RING), S, 2 * cap, D), b16),
             pltpu.VMEM((Z, S, 2 * cap, D), b16),
             pltpu.VMEM((Z, S, 2 * cap, D), b16),
+            pltpu.VMEM((Z, rows, D), b16),
             pltpu.VMEM((Z, rows, D), b16),
             pltpu.VMEM((Z, rows, D), b16),
             pltpu.VMEM((2, rows, D), f32),
@@ -558,21 +671,25 @@
             dma((2,)), dma((2,)),
             dma((S - 1,)), dma((S - 1,)),
             dma((T,)), dma((T,)),
-            dma((max(L - 1, 1), 3)), dma((max(L - 1, 1), 3)),
+            dma((4, 2)), dma((4, 4)),
+            dma((3,)), dma((3,)),
             dma((2, Z)), dma((Z,)),
             dma((Z,)), dma((Z,)),
             dma((Z, S - 1)), dma((Z, S - 1)),
             dma((Z, S - 1)), dma((Z, S - 1)),
             dma((Z,)), dma((Z,)),
             dma((Z,)), dma((Z,)),
+            dma((Z,)), dma((Z,)),
         ],
         compiler_params=pltpu.CompilerParams(
-            collective_id=0, has_side_effects=True, vmem_limit_bytes=62 * 1024 * 1024
+            collective_id=0, has_side_effects=True, vmem_limit_bytes=63 * 1024 * 1024
         ),
     )(
-        mix_in, gate_in, conv_w, conv_b.reshape(1, C), soft, recur_gate, recur_bias, input_gate,
-        input_bias, residual, norm_gain, sel, comb, weights, out_proj, exp_gate, exp_up, exp_down,
+        mix_in, gate_in, conv_w, conv_b.reshape(1, C), decay_param, recur_gate, recur_bias,
+        input_gate, input_bias, residual, norm_gain, routes.T, route_wt.T, out_proj,
+        exp_gate, exp_up, exp_down,
     )
+    return (stream.astype(f32) + delta).astype(b16)
 
 
 def solution(mesh):

time: 207 us -> 179 us (0.86)
  Pallas kernels: 199 us -> 177 us
  local copies, waits for them, and re-layouts: 5.97 us -> 0 us
    pallas_call x1, Pallas kernels: 199 us -> 177 us  [on_device(): pl.pallas_call(functools.partial(layer_kernel, dims), out_shape=(jax.Shap...]
    unnamed x7 -> x0, local copies, waits for them, and re-layouts: 3.83 us -> none
    convert_element_type x0 -> x1, other arithmetic: none -> 2.26 us  [on_device(): return (stream.astype(f32) + delta).astype(b16)]
where the time goes in v2:
time: 179 us
  Pallas kernels  177 us (99%)
  other arithmetic  2.26 us (1%)
    pallas_call x1, Pallas kernels, on_device(): pl.pallas_call(functools.partial(layer_kernel, dims), out_shape=(jax.Shap...  177 us

profile of v2, /device:TPU:0, one launch (start us, length us, event | category | flops | bytes accessed | tf_op | source)
XLA Modules:
  0.0 178.9 jit_solution(301089666925361781)
XLA Ops:
  0.0 176.7 %shard_map.163 = (bf16[128,2048]{1,0:T(8,128)(2,1)}, f32[128,2048]{1,0:T(8,128)}) custom-call(bf16[1024,256]{1,0:T(8,128)(2,1)} %mix_ref.1, bf16[1024,256]{1,0:T(8,128)(2,1)} %gate_ref.1, f32[4,256]{1,0:T(4,128)} %cw_ref.1, f32[1,256]{1,0:T(1,128)} %bitcast.5, f32[2,256]{1,0:T(2,128)} %decay_ref.1, f32[2,4,64,64]{3,2,1,0:T(8,128)} %rg_ref.1, ...), custom_call_target="tpu_custom_call" | custom-call | tf_op jit(solution)/shard_map/pallas_call | solution.py:641
  176.7 2.3 %add_convert_fusion = bf16[128,2048]{1,0:T(8,128)(2,1)} fusion(f32[128,2048]{1,0:T(8,128)} %get-tuple-element.8, bf16[128,2048]{1,0:T(8,128)(2,1)} %get-tuple-element.7), kind=kLoop, calls=%fused_computation | loop fusion | flops 786432 | bytes 2097152 | tf_op jit(solution)/shard_map/convert_element_type | solution.py:692

commit v3 on v2

--- a/solution.py
+++ b/solution.py
@@ -331,9 +331,13 @@
         return remote(gath.at[2 * zc + 1 - g], prem.at[zc], pd_send.at[zc], pd_recv.at[zc],
                       sp, partner)
 
-    def deliver(zc):
-        return remote(gath.at[2 * zc + g], zrec.at[z], zs_send.at[zc], zs_recv.at[z],
-                      sp, 2 * zc + g)
+    def half_at(h):
+        return pl.ds(h * (rows // 2), rows // 2)
+
+    def deliver(zc, h):
+        at = half_at(h)
+        return remote(gath.at[2 * zc + g, at], zrec.at[z, at], zs_send.at[zc, h],
+                      zs_recv.at[z, h], sp, 2 * zc + g)
 
     def slot_table(zc, weighted):
         at = pl.ds(pl.multiple_of(zc * (2 * rows), 2 * rows), 2 * rows)
@@ -416,15 +420,13 @@
         cols = pl.ds(pl.multiple_of(n * pair_width, pair_width), pair_width)
         if L == 1:
             cols = slice(None)
-        hid[j, :, cols] = activate(arr[zc].reshape(slots, D), wg[:, cols], wu[:, cols])
-
-    def down_part(j, depth):
-        zc = chip_at(j)
-
+        hid[zc, :, cols] = activate(arr[zc].reshape(slots, D), wg[:, cols], wu[:, cols])
+
+    def down_part(zc, depth):
         def down(n, _):
             cols = pl.ds(pl.multiple_of(n * wide, wide), wide)
             rows_out = jnp.dot(
-                hid[j, :, :depth], wd[:depth, cols], preferred_element_type=jnp.float32
+                hid[zc, :, :depth], wd[:depth, cols], preferred_element_type=jnp.float32
             )
             arr[zc, :, :, cols] = rows_out.astype(jnp.bfloat16).reshape(S, two_cap, wide)
             return 0
@@ -437,6 +439,9 @@
 
     early = middle & (g == 0)
 
+    def return_order(i):
+        return chip_at(lax.rem(i + 1, Z))
+
     def stage(j, _):
         @pl.when(j < Z)
         def _():
@@ -464,7 +469,7 @@
 
             @pl.when(jnp.logical_not(middle))
             def _():
-                down_part(j - 1, pair_width)
+                down_part(chip_at(j - 1), pair_width)
 
                 @pl.when(j > 1)
                 def _():
@@ -495,16 +500,13 @@
             weights_arrived((3,))
 
             def finish_rows(i, _):
-                down_part(Z - 1 - i, 3 * pair_width)
-                return_rows(chip_at(Z - 1 - i))
+                down_part(return_order(i), 3 * pair_width)
+                return_rows(return_order(i))
                 return 0
 
             lax.fori_loop(0, Z, finish_rows, 0)
 
     pair_chip = z + 1 - 2 * lax.rem(z, 2)
-
-    def return_order(i):
-        return chip_at(jnp.where(middle, Z - 1 - i, lax.rem(i + 1, Z)))
 
     def feeds(zc):
         return (zc != z) & (zc != pair_chip) & ((zc > z) == (lax.rem(z, 2) == 0))
@@ -512,9 +514,10 @@
     def relays(zc):
         return (zc != z) & (zc != pair_chip) & ((zc > z) != (lax.rem(z, 2) == 0))
 
-    def feed(zc):
-        return remote(gath.at[2 * zc + g], pin.at[zc], pin_send.at[zc], pin_recv.at[zc],
-                      sp, 2 * pair_chip + g)
+    def feed(zc, h):
+        at = half_at(h)
+        return remote(gath.at[2 * zc + g, at], pin.at[zc, at], pin_send.at[zc, h],
+                      pin_recv.at[zc, h], sp, 2 * pair_chip + g)
 
     def combine(i, _):
         zc = return_order(i)
@@ -528,11 +531,11 @@
         def _():
             along(zc, 1).wait_send()
 
+        table = jnp.transpose(slot_table(zc, True))
+        high, low = split_f32(table)
         for ds in range(1, S):
             give_back(zc, ds).wait_recv()
         back[zc, sp] = arr[zc, sp]
-        table = jnp.transpose(slot_table(zc, True))
-        high, low = split_f32(table)
 
         def mix(n, _):
             cols = pl.ds(pl.multiple_of(n * wide, wide), wide)
@@ -547,39 +550,43 @@
         merge(zc).start()
         merge(zc).wait_recv()
 
-        @pl.when(feeds(zc) | (zc == pair_chip))
-        def _():
-            gath[2 * zc + g] = (pbuf[g] + prem[zc].astype(jnp.float32)).astype(jnp.bfloat16)
-
-        @pl.when(feeds(zc))
-        def _():
-            feed(zc).start()
-
-        @pl.when(relays(zc))
-        def _():
-            pltpu.make_async_copy(pin.at[zc], pin.at[zc], pin_recv.at[zc]).wait()
-            gath[2 * zc + g] = (
-                pbuf[g] + prem[zc].astype(jnp.float32) + pin[zc].astype(jnp.float32)
-            ).astype(jnp.bfloat16)
-            deliver(zc).start()
-
-        @pl.when(zc == pair_chip)
-        def _():
-            deliver(zc).start()
+        for h in range(2):
+            at = half_at(h)
+
+            @pl.when(relays(zc))
+            def _():
+                pltpu.make_async_copy(pin.at[zc, at], pin.at[zc, at], pin_recv.at[zc, h]).wait()
+                gath[2 * zc + g, at] = (
+                    pbuf[g, at] + prem[zc, at].astype(jnp.float32)
+                    + pin[zc, at].astype(jnp.float32)
+                ).astype(jnp.bfloat16)
+
+            @pl.when(feeds(zc) | (zc == pair_chip))
+            def _():
+                gath[2 * zc + g, at] = (
+                    pbuf[g, at] + prem[zc, at].astype(jnp.float32)
+                ).astype(jnp.bfloat16)
+
+            @pl.when(feeds(zc))
+            def _():
+                feed(zc, h).start()
+
+            @pl.when(relays(zc) | (zc == pair_chip))
+            def _():
+                deliver(zc, h).start()
 
         return 0
 
     lax.fori_loop(0, Z, combine, 0)
-
-    def arrived(zc):
-        return pltpu.make_async_copy(zrec.at[zc], zrec.at[zc], zs_recv.at[zc])
 
     senders = [pair_chip]
     for m in range(1, Z // 2):
         other = lax.rem(lax.div(z, 2) + m, Z // 2)
         senders.append(2 * other + jnp.where(2 * other < z, 1, 0))
     for zc in senders:
-        arrived(zc).wait()
+        for h in range(2):
+            block = zrec.at[zc, half_at(h)]
+            pltpu.make_async_copy(block, block, zs_recv.at[zc, h]).wait()
 
     def finish(n, _):
         at = pl.ds(pl.multiple_of(n * part, part), part)
@@ -610,11 +617,13 @@
 
         @pl.when(feeds(zc))
         def _():
-            feed(zc).wait_send()
+            for h in range(2):
+                feed(zc, h).wait_send()
 
         @pl.when((zc != z) & jnp.logical_not(feeds(zc)))
         def _():
-            deliver(zc).wait_send()
+            for h in range(2):
+                deliver(zc, h).wait_send()
 
         return 0
 
@@ -678,8 +687,8 @@
             dma((Z, S - 1)), dma((Z, S - 1)),
             dma((Z, S - 1)), dma((Z, S - 1)),
             dma((Z,)), dma((Z,)),
-            dma((Z,)), dma((Z,)),
-            dma((Z,)), dma((Z,)),
+            dma((Z, 2)), dma((Z, 2)),
+            dma((Z, 2)), dma((Z, 2)),
         ],
         compiler_params=pltpu.CompilerParams(
             collective_id=0, has_side_effects=True, vmem_limit_bytes=63 * 1024 * 1024

time: 179 us -> 169 us (0.944)
  the two profiles are of different devices: /device:TPU:0 before, /device:TPU:27 now
where the time goes in v3:
time: 169 us
  Pallas kernels  167 us (99%)
  other arithmetic  2.26 us (1%)
    pallas_call x1, Pallas kernels, on_device(): pl.pallas_call(functools.partial(layer_kernel, dims), out_shape=(jax.Shap...  167 us

profile of v3, /device:TPU:27, one launch (start us, length us, event | category | flops | bytes accessed | tf_op | source)
XLA Modules:
  0.0 168.9 jit_solution(18066547260639893997)
XLA Ops:
  0.0 166.6 %shard_map.163 = (bf16[128,2048]{1,0:T(8,128)(2,1)}, f32[128,2048]{1,0:T(8,128)}) custom-call(bf16[1024,256]{1,0:T(8,128)(2,1)} %mix_ref.1, bf16[1024,256]{1,0:T(8,128)(2,1)} %gate_ref.1, f32[4,256]{1,0:T(4,128)} %cw_ref.1, f32[1,256]{1,0:T(1,128)} %bitcast.5, f32[2,256]{1,0:T(2,128)} %decay_ref.1, f32[2,4,64,64]{3,2,1,0:T(8,128)} %rg_ref.1, ...), custom_call_target="tpu_custom_call" | custom-call | tf_op jit(solution)/shard_map/pallas_call | solution.py:650
  166.6 2.3 %add_convert_fusion = bf16[128,2048]{1,0:T(8,128)(2,1)} fusion(f32[128,2048]{1,0:T(8,128)} %get-tuple-element.8, bf16[128,2048]{1,0:T(8,128)(2,1)} %get-tuple-element.7), kind=kLoop, calls=%fused_computation | loop fusion | flops 786432 | bytes 2097152 | tf_op jit(solution)/shard_map/convert_element_type | solution.py:701

commit v4 on v3

--- a/solution.py
+++ b/solution.py
@@ -438,9 +438,13 @@
             give_back(zc, ds).start()
 
     early = middle & (g == 0)
+    pair_chip = z + 1 - 2 * lax.rem(z, 2)
 
     def return_order(i):
-        return chip_at(lax.rem(i + 1, Z))
+        pair_at = jnp.where((lax.rem(z, 2) == 1) | (z == 0), 1, 2)
+        others = jnp.where(i + 1 < pair_at, i + 1, i + 2)
+        ordered = jnp.where(i < Z - 2, others, jnp.where(i == Z - 2, pair_at, 0))
+        return chip_at(jnp.where(middle, lax.rem(i + 1, Z), ordered))
 
     def stage(j, _):
         @pl.when(j < Z)
@@ -471,7 +475,7 @@
             def _():
                 down_part(chip_at(j - 1), pair_width)
 
-                @pl.when(j > 1)
+                @pl.when((j > 1) & (chip_at(j - 1) != pair_chip))
                 def _():
                     return_rows(chip_at(j - 1))
 
@@ -481,6 +485,7 @@
 
     @pl.when(jnp.logical_not(middle))
     def _():
+        return_rows(pair_chip)
         return_rows(z)
 
     if L > 1:
@@ -506,7 +511,6 @@
 
             lax.fori_loop(0, Z, finish_rows, 0)
 
-    pair_chip = z + 1 - 2 * lax.rem(z, 2)
 
     def feeds(zc):
         return (zc != z) & (zc != pair_chip) & ((zc > z) == (lax.rem(z, 2) == 0))

time: 169 us -> 163 us (0.964)
  the two profiles are of different devices: /device:TPU:27 before, /device:TPU:0 now
where the time goes in v4:
time: 163 us; the launch traced here: 161 us
  Pallas kernels  159 us (98%)
  other arithmetic  2.26 us (1%)
    pallas_call x1, Pallas kernels, on_device(): pl.pallas_call(functools.partial(layer_kernel, dims), out_shape=(jax.Shap...  159 us

profile of v4, /device:TPU:0, one launch (start us, length us, event | category | flops | bytes accessed | tf_op | source)
XLA Modules:
  0.0 161.3 jit_solution(708249047312072806)
XLA Ops:
  0.0 159.1 %shard_map.163 = (bf16[128,2048]{1,0:T(8,128)(2,1)}, f32[128,2048]{1,0:T(8,128)}) custom-call(bf16[1024,256]{1,0:T(8,128)(2,1)} %mix_ref.1, bf16[1024,256]{1,0:T(8,128)(2,1)} %gate_ref.1, f32[4,256]{1,0:T(4,128)} %cw_ref.1, f32[1,256]{1,0:T(1,128)} %bitcast.5, f32[2,256]{1,0:T(2,128)} %decay_ref.1, f32[2,4,64,64]{3,2,1,0:T(8,128)} %rg_ref.1, ...), custom_call_target="tpu_custom_call" | custom-call | tf_op jit(solution)/shard_map/pallas_call | solution.py:654
  159.1 2.3 %add_convert_fusion = bf16[128,2048]{1,0:T(8,128)(2,1)} fusion(f32[128,2048]{1,0:T(8,128)} %get-tuple-element.8, bf16[128,2048]{1,0:T(8,128)(2,1)} %get-tuple-element.7), kind=kLoop, calls=%fused_computation | loop fusion | flops 786432 | bytes 2097152 | tf_op jit(solution)/shard_map/convert_element_type | solution.py:705
